TPU v7x, 32 devices: a whole 2x2x4 slice. The times are simulated.
32 devices in a mesh: ep: 8 (over z, x), tp: 4 (over y, core).
Axes of the slice: x: 2, y: 2, z: 4, core: 2. Of those that a mesh axis runs over, the one named last changes fastest.
Arguments:
- tokens: bfloat16 [384, 1024], P('ep'), may hold values from -6 to 6
- head_state: float32 [384, 8, 64, 64], P('ep', 'tp'), may hold values from -6 to 6
- recept_weight: bfloat16 [1024, 512], P(None, 'tp'), may hold values from -0.1875 to 0.1875
- key_weight: bfloat16 [1024, 512], P(None, 'tp'), may hold values from -0.1875 to 0.1875
- value_weight: bfloat16 [1024, 512], P(None, 'tp'), may hold values from -0.1875 to 0.1875
- decay_down_factor: bfloat16 [1024, 64], replicated, may hold values from -0.1875 to 0.1875
- decay_up_factor: bfloat16 [64, 512], P(None, 'tp'), may hold values from -0.75 to 0.75
- decay_base: float32 [512], P('tp'), may hold values from -5 to 3
- rate_down_factor: bfloat16 [1024, 64], replicated, may hold values from -0.1875 to 0.1875
- rate_up_factor: bfloat16 [64, 512], P(None, 'tp'), may hold values from -0.75 to 0.75
- rate_base: float32 [512], P('tp'), may hold values from -3 to 3
- head_gain: float32 [512], P('tp'), may hold values from 0.1 to 1.9
- out_weight: bfloat16 [512, 1024], P('tp'), may hold values from -0.25 to 0.25
- route_experts: int32 [384, 4], P('ep'), may hold values from 0 to 7, all different within a row; in each aligned block of 48 rows (0 to 47, 48 to 95, ...) at most 48 rows name the same one
- route_weights: float32 [384, 4], P('ep'), may hold values from 0.03 to 0.2
- expert_gate: bfloat16 [8, 1024, 1024], P('ep', None, 'tp'), may hold values from -1 to 1
- expert_up: bfloat16 [8, 1024, 1024], P('ep', None, 'tp'), may hold values from -1 to 1
- expert_down: bfloat16 [8, 1024, 1024], P('ep', 'tp'), may hold values from -0.1875 to 0.1875
Outputs:
- layer_out: bfloat16 [384, 1024], P('ep', 'tp')
- new_state: float32 [384, 8, 64, 64], P('ep', 'tp')
Inputs may be any that keep to these rules, and one draw needn't show every extreme that they name: `route_experts`: each row names 4 different experts. In each aligned block of 48 rows no expert is named by more than 48 rows, a bound that some block reaches.
All inputs are finite; a program needn't handle non-finite values.
Results may differ from a plain program's by a relative error of at most 0.02.
Values may be sent and summed in bfloat16 or wider, within the bound.
No kernel may reach another device: no remote copies, remote signals or barrier semaphores. Data moves between devices by JAX's collectives and lax.ppermute only.
A program may use at most 128 MiB of HBM per device.

v0:
```python
import jax
import jax.numpy as jnp
from jax import lax
from jax.sharding import PartitionSpec as P

NORM_EPS = 1e-05
GROUP_EPS = 0.00064
UNIT_EPS = 1e-06
CLAMP_LIMIT = 7.0
GLU_ALPHA = 1.702


def row_norm(values):
    return values * lax.rsqrt(jnp.mean(values * values, axis=-1, keepdims=True) + NORM_EPS)


def clamped_unit(gate_pre, up_pre):
    gated = jnp.minimum(gate_pre, CLAMP_LIMIT)
    linear = jnp.clip(up_pre, -CLAMP_LIMIT, CLAMP_LIMIT)
    return gated * jax.nn.sigmoid(GLU_ALPHA * gated) * (linear + 1.0)


def update_heads(head_state, recept, keys, values, decay_rate, rate_gate, head_gain):
    seq_count, head_count, head_size = head_state.shape[:3]

    def by_heads(operand):
        return operand.astype(jnp.float32).reshape(seq_count, head_count, head_size)

    recept_heads = by_heads(recept)
    key_heads = by_heads(keys)
    value_heads = by_heads(values)
    decay_heads = by_heads(decay_rate)
    rate_heads = by_heads(rate_gate)
    unit_key = key_heads * lax.rsqrt(
        jnp.sum(key_heads * key_heads, axis=-1, keepdims=True) + UNIT_EPS
    )
    highest = lax.Precision.HIGHEST
    state_unit = jnp.einsum("shvk,shk->shv", head_state, unit_key, precision=highest)
    new_state = (
        head_state * decay_heads[:, :, None, :]
        - state_unit[..., None] * (unit_key * rate_heads)[:, :, None, :]
        + value_heads[..., None] * (key_heads * rate_heads)[:, :, None, :]
    )
    head_out = jnp.einsum("shvk,shk->shv", new_state, recept_heads, precision=highest)
    centre = jnp.mean(head_out, axis=-1, keepdims=True)
    spread = jnp.mean(jnp.square(head_out - centre), axis=-1, keepdims=True)
    normed_heads = (head_out - centre) * lax.rsqrt(spread + GROUP_EPS)
    mixed = (normed_heads.reshape(seq_count, -1) * head_gain).astype(jnp.bfloat16)
    return (new_state, mixed)


def local(
    tokens,
    head_state,
    recept_weight,
    key_weight,
    value_weight,
    decay_down_factor,
    decay_up_factor,
    decay_base,
    rate_down_factor,
    rate_up_factor,
    rate_base,
    head_gain,
    out_weight,
    route_experts,
    route_weights,
    expert_gate,
    expert_up,
    expert_down,
):
    tokens_float = tokens.astype(jnp.float32)
    normed = row_norm(tokens_float).astype(jnp.bfloat16)
    recept = jnp.dot(normed, recept_weight, preferred_element_type=jnp.float32).astype(jnp.bfloat16)
    keys = jnp.dot(normed, key_weight, preferred_element_type=jnp.float32).astype(jnp.bfloat16)
    values = jnp.dot(normed, value_weight, preferred_element_type=jnp.float32).astype(jnp.bfloat16)
    decay_low = jnp.tanh(
        jnp.dot(normed, decay_down_factor, preferred_element_type=jnp.float32)
    ).astype(jnp.bfloat16)
    rate_low = jnp.dot(normed, rate_down_factor, preferred_element_type=jnp.float32).astype(
        jnp.bfloat16
    )
    decay_pre = decay_base + jnp.dot(decay_low, decay_up_factor, preferred_element_type=jnp.float32)
    decay_rate = jnp.exp(-jnp.exp(-jax.nn.softplus(-decay_pre) - 0.5))
    rate_gate = jax.nn.sigmoid(
        rate_base + jnp.dot(rate_low, rate_up_factor, preferred_element_type=jnp.float32)
    )
    new_state, mixed = update_heads(
        head_state, recept, keys, values, decay_rate, rate_gate, head_gain
    )
    partial_value = jnp.dot(mixed, out_weight, preferred_element_type=jnp.float32).astype(
        jnp.bfloat16
    )
    partial_value = lax.optimization_barrier(partial_value).astype(jnp.float32)
    summed = lax.psum(partial_value.astype(jnp.bfloat16), "tp").astype(jnp.float32)
    residual = (tokens_float + summed).astype(jnp.bfloat16)
    expert_input = row_norm(residual.astype(jnp.float32)).astype(jnp.bfloat16)
    seq_count, top_count = route_experts.shape
    expert_count = lax.axis_size("ep")
    capacity = max(2, (2 * seq_count * top_count + expert_count - 1) // expert_count)
    column_count = expert_input.shape[1] // lax.axis_size("tp")
    column_start = lax.axis_index("tp") * column_count
    flat_routes = route_experts.reshape(-1)
    onehot = (flat_routes[:, None] == jnp.arange(expert_count, dtype=jnp.int32)[None, :]).astype(
        jnp.int32
    )
    earlier = jnp.cumsum(onehot, axis=0) - onehot
    target = flat_routes * capacity + jnp.sum(earlier * onehot, axis=1)
    slot_ids = jnp.arange(expert_count * capacity, dtype=jnp.int32)
    dispatch_map = jnp.any(
        slot_ids[:, None, None] == target.reshape(seq_count, top_count)[None], axis=-1
    )
    dispatch_map = dispatch_map.astype(jnp.bfloat16)
    outgoing = lax.dynamic_slice_in_dim(expert_input, column_start, column_count, 1)
    buffer = jnp.dot(dispatch_map, outgoing, preferred_element_type=jnp.float32).astype(
        jnp.bfloat16
    )
    buffer = buffer.reshape(expert_count, capacity, outgoing.shape[1])
    slot_rows = lax.all_gather(
        lax.all_to_all(buffer, "ep", split_axis=0, concat_axis=0, tiled=True),
        "tp",
        axis=2,
        tiled=True,
    )
    source_count, slot_count, model_width = slot_rows.shape
    flat_rows = slot_rows.reshape(-1, model_width)
    gate_pre = jnp.dot(flat_rows, expert_gate[0], preferred_element_type=jnp.float32)
    up_pre = jnp.dot(flat_rows, expert_up[0], preferred_element_type=jnp.float32)
    activated = clamped_unit(gate_pre, up_pre).astype(jnp.bfloat16)
    part_out = jnp.dot(activated, expert_down[0], preferred_element_type=jnp.float32).astype(
        jnp.bfloat16
    )
    part_out = lax.optimization_barrier(part_out).astype(jnp.float32)
    part_out = part_out.reshape(source_count, slot_count, model_width)
    shares = lax.psum_scatter(part_out.astype(jnp.bfloat16), "tp", scatter_dimension=2, tiled=True)
    returned = lax.all_to_all(shares, "ep", split_axis=0, concat_axis=0, tiled=True)
    picked = returned.reshape(expert_count * capacity, column_count)[target]
    picked = picked.reshape(seq_count, top_count, column_count).astype(jnp.float32)
    mixture = jnp.sum(route_weights[:, :, None] * picked, axis=1)
    own_residual = lax.dynamic_slice_in_dim(residual, column_start, column_count, 1).astype(
        jnp.float32
    )
    layer_out = (own_residual + mixture).astype(jnp.bfloat16)
    return (layer_out, new_state)


def solution(mesh):
    in_specs = (
        P("ep", None),
        P("ep", "tp", None, None),
        P(None, "tp"),
        P(None, "tp"),
        P(None, "tp"),
        P(),
        P(None, "tp"),
        P("tp"),
        P(),
        P(None, "tp"),
        P("tp"),
        P("tp"),
        P("tp", None),
        P("ep", None),
        P("ep", None),
        P("ep", None, "tp"),
        P("ep", None, "tp"),
        P("ep", "tp", None),
    )
    out_specs = (P("ep", "tp"), P("ep", "tp", None, None))
    return jax.shard_map(local, mesh=mesh, in_specs=in_specs, out_specs=out_specs, check_vma=False)
```

profile of v0, /device:TPU:0, one launch (start us, length us, event | category | flops | bytes accessed | tf_op | source)
XLA Modules:
  0.0 132.7 jit_solution(9616172341950078391)
XLA Ops:
  7.2 1.1 fusion.22
  8.3 1.2 fusion.10
  9.8 1.3 %fusion.6 = f32[48,128]{1,0:T(8,128)S(1)} fusion(bf16[64,128]{1,0:T(8,128)(2,1)} %param.27, bf16[1024,64]{0,1:T(8,128)(2,1)} %param.26, f32[128]{0:T(128)} %param.28, bf16[48,1024]{1,0:T(8,128)(2,1)} %param.18, f32[48]{0:T(128)S(1)} %add_rsqrt_fusion.3), kind=kOutput, calls=%fused_computation.14 | convolution fusion | flops 7252992 | bytes 271040 | tf_op jit(solution)/shard_map/dot_general | solution.py:86
  11.2 1.4 %fusion.35 = f32[48,128]{1,0:T(8,128)S(1)} fusion(bf16[64,128]{1,0:T(8,128)(2,1)} %param.24, bf16[1024,64]{0,1:T(8,128)(2,1)} %param.23, f32[128]{0:T(128)} %param.25, bf16[48,1024]{1,0:T(8,128)(2,1)} %param.18, f32[48]{0:T(128)S(1)} %add_rsqrt_fusion.3), kind=kOutput, calls=%fused_computation.59 | convolution fusion | flops 7296000 | bytes 271040 | tf_op jit(solution)/shard_map/dot_general | solution.py:83
  12.7 1.2 fusion.9
  14.0 1.2 convolution_convert_fusion.3
  15.5 7.0 %fusion.55 = f32[48,2,1,64]{3,2,1,0:T(1,128)S(1)} fusion(f32[48,2,64,1]{2,3,1,0:T(1,128)S(1)} %bitcast.53, f32[48,2,64,64]{3,2,1,0:T(8,128)} %param.19), kind=kOutput, calls=%fused_computation.87 | convolution fusion | flops 4718592 | bytes 1622016 | tf_op jit(solution)/shard_map/shvk,shk->shv/dot_general | solution.py:38
  22.5 2.1 %multiply_add_fusion = f32[48,2,64,64]{3,2,1,0:T(8,128)S(1)} fusion(f32[48,2,64,64]{3,2,1,0:T(8,128)S(1)} %copy-done.1, f32[48,2,64]{2,1,0:T(2,128)S(1)} %get-tuple-element.6, f32[48,2,64]{2,1,0:T(2,128)S(1)} %reshape.152, f32[48,2,64]{2,1,0:T(2,128)S(1)} %get-tuple-element.4, f32[48,2,64]{2,1,0:T(2,128)S(1)} %bitcast.52, f32[48,2,64]{2,1,0:T(2,128)S(1)} %mul.155), kind=kLoop, calls=%fused_computation.1 | loop fusion | flops 1966080 | bytes 3268608 | tf_op jit(solution)/shard_map/add | solution.py:40
  24.6 1.7 %copy-done.2 = f32[48,2,64,64]{3,2,1,0:T(8,128)} copy-done((f32[48,2,64,64]{3,2,1,0:T(8,128)}, f32[48,2,64,64]{3,2,1,0:T(8,128)S(1)}, u32[]{:S(2)}) %copy-start.2) | copy-done | bytes 1572888
  26.2 2.5 %fusion.56 = f32[48,2,1,64]{3,2,1,0:T(1,128)S(1)} fusion(f32[48,2,64,64]{3,2,1,0:T(8,128)S(1)} %multiply_add_fusion, bf16[48,2,64,1]{2,3,1,0:T(2,128)(2,1)S(1)} %reshape.168), kind=kOutput, calls=%fused_computation.88 | convolution fusion | flops 4718592 | bytes 1609728 | tf_op jit(solution)/shard_map/shvk,shk->shv/dot_general | solution.py:44
  29.4 0.8 convolution_convert_fusion.2
  30.6 0.6 reduce-window.6
  31.8 33.0 %all-reduce.3.cloned.1.call-done = bf16[48,1024]{1,0:T(8,128)(2,1)} async-done(((bf16[48,1024]{1,0:T(8,128)(2,1)}), bf16[48,1024]{1,0:T(8,128)(2,1)}) %all-reduce.3.cloned.1.call-update) | async-done | bytes 98320 | tf_op jit(solution)/shard_map/psum | solution.py:95
  64.8 1.0 multiply_reduce_fusion.1
  65.9 0.3 convolution_convert_fusion.1
  66.2 13.1 %all_to_all.10 = bf16[8,48,256]{2,1,0:T(8,128)(2,1)S(1)} all-to-all(bf16[8,48,256]{2,1,0:T(8,128)(2,1)S(1)} %bitcast.48), channel_id=1, replica_groups=mesh['ep'=8,'tp'=4] {'ep'}, dimensions={0} | all-to-all | bytes 393216 | tf_op jit(solution)/shard_map/all_to_all | solution.py:120
  79.3 7.6 %all_gather.3 = bf16[8,48,1024]{2,1,0:T(8,128)(2,1)S(1)} all-gather(bf16[8,48,256]{2,1,0:T(8,128)(2,1)S(1)} %all_to_all.10), channel_id=1, replica_groups=mesh['ep'=8,'tp'=4] {'tp'}, dimensions={2}, use_global_device_ids=true | all-gather | bytes 983040 | tf_op jit(solution)/shard_map/all_gather | solution.py:119
  86.9 0.4 convolution_minimum_fusion
  87.3 1.9 %convolution_convert_fusion = bf16[384,1024]{1,0:T(8,128)(2,1)} fusion(bf16[384,1024]{1,0:T(8,128)(2,1)S(1)} %bitcast.46, bf16[1,256,1024]{2,1,0:T(8,128)(2,1)S(1)} %copy-done, bf16[1,1024,256]{2,1,0:T(8,128)(2,1)S(1)} %copy-done.9, f32[384,256]{1,0:T(8,128)S(1)} %convolution_minimum_fusion), kind=kOutput, calls=%fused_computation.2 | convolution fusion | flops 403931136 | bytes 3014656 | tf_op jit(solution)/shard_map/dot_general | solution.py:130
  89.2 21.5 %reduce-scatter.2.cloned.1.call-done = bf16[8,48,256]{2,1,0:T(8,128)(2,1)} async-done(((bf16[8,48,1024]{2,1,0:T(8,128)(2,1)}), bf16[8,48,256]{2,1,0:T(8,128)(2,1)}) %reduce-scatter.2.cloned.1.call-update) | async-done | bytes 196624 | tf_op jit(solution)/shard_map/reduce_scatter | solution.py:135
  110.6 5.5 %all-to-all-start.1 = ((bf16[8,48,256]{2,1,0:T(8,128)(2,1)}), bf16[8,48,256]{2,1,0:T(8,128)(2,1)S(1)}, u32[]{:S(2)}, u32[]{:S(2)}) async-start(bf16[8,48,256]{2,1,0:T(8,128)(2,1)} %reduce-scatter.2.cloned.1.call-done), calls=%async_computation.2 | async-start | bytes 393216 | tf_op jit(solution)/shard_map/all_to_all | solution.py:136
  116.4 7.6 %all-to-all-done.1 = bf16[8,48,256]{2,1,0:T(8,128)(2,1)S(1)} async-done(((bf16[8,48,256]{2,1,0:T(8,128)(2,1)}), bf16[8,48,256]{2,1,0:T(8,128)(2,1)S(1)}, u32[]{:S(2)}, u32[]{:S(2)}) %all-to-all-start.1) | async-done | bytes 196640 | tf_op jit(solution)/shard_map/all_to_all | solution.py:136
  123.9 1.0 gather_fusion
  125.2 0.6 add_convert_fusion
  (59 shorter events, 2.8 us)
Async XLA Ops:
  7.2 80.1 %copy-start = (bf16[1,256,1024]{2,1,0:T(8,128)(2,1)S(1)}, bf16[1,256,1024]{2,1,0:T(8,128)(2,1)}, u32[]{:S(2)}) copy-start(bf16[1,256,1024]{2,1,0:T(8,128)(2,1)} %param.35) | copy-start | bytes 1572868
  7.2 57.6 %all-reduce.3.cloned.1.call-start = ((), (), s32[]{:S(2)}) async-start(), calls=%async_computation.3 | async-start | bytes 196608 | tf_op jit(solution)/shard_map/psum | solution.py:95
  15.3 7.2 %copy-start.1 = (f32[48,2,64,64]{3,2,1,0:T(8,128)S(1)}, f32[48,2,64,64]{3,2,1,0:T(8,128)}, u32[]{:S(2)}) copy-start(f32[48,2,64,64]{3,2,1,0:T(8,128)} %param.19) | copy-start | bytes 4718596
  24.6 1.7 %copy-start.2 = (f32[48,2,64,64]{3,2,1,0:T(8,128)}, f32[48,2,64,64]{3,2,1,0:T(8,128)S(1)}, u32[]{:S(2)}) copy-start(f32[48,2,64,64]{3,2,1,0:T(8,128)S(1)} %multiply_add_fusion) | copy-start | bytes 4718596
  26.2 3.2 %copy-start.5 = (bf16[128,1024]{1,0:T(8,128)(2,1)S(1)}, bf16[128,1024]{1,0:T(8,128)(2,1)}, u32[]{:S(2)}) copy-start(bf16[128,1024]{1,0:T(8,128)(2,1)} %param.30) | copy-start | bytes 786436
  26.2 3.2 %copy-start.8 = (f32[128]{0:T(128)S(1)}, f32[128]{0:T(128)}, u32[]{:S(2)}) copy-start(f32[128]{0:T(128)} %param.29) | copy-start | bytes 1540
  26.2 4.1 %copy-start.6 = (s32[48,4]{0,1:T(4,128)S(1)}, s32[48,4]{0,1:T(4,128)}, u32[]{:S(2)}) copy-start(s32[48,4]{0,1:T(4,128)} %param.31) | copy-start | bytes 2308
  26.2 38.6 %copy-start.3 = (bf16[48,1024]{1,0:T(8,128)(2,1)S(1)}, bf16[48,1024]{1,0:T(8,128)(2,1)}, u32[]{:S(2)}) copy-start(bf16[48,1024]{1,0:T(8,128)(2,1)} %param.18) | copy-start | bytes 294916
  26.2 60.6 %copy-start.4 = (bf16[1,1024,256]{2,1,0:T(8,128)(2,1)S(1)}, bf16[1,1024,256]{2,1,0:T(8,128)(2,1)}, u32[]{:S(2)}) copy-start(bf16[1,1024,256]{2,1,0:T(8,128)(2,1)} %param.33) | copy-start | bytes 1572868
  28.8 58.5 %copy-start.9 = (bf16[1,1024,256]{2,1,0:T(8,128)(2,1)S(1)}, bf16[1,1024,256]{2,1,0:T(8,128)(2,1)}, u32[]{:S(2)}) copy-start(bf16[1,1024,256]{2,1,0:T(8,128)(2,1)} %param.34) | copy-start | bytes 1572868
  30.3 80.4 %reduce-scatter.2.cloned.1.call-start = ((), (), s32[]{:S(2)}) async-start(), calls=%async_computation.4 | async-start | bytes 983040 | tf_op jit(solution)/shard_map/reduce_scatter | solution.py:135
  87.3 29.0 %copy-start.7 = (f32[48,4]{0,1:T(4,128)S(1)}, f32[48,4]{0,1:T(4,128)}, u32[]{:S(2)}) copy-start(f32[48,4]{0,1:T(4,128)} %param.32) | copy-start | bytes 2308
  110.6 13.3 %all-to-all-start.1 = ((bf16[8,48,256]{2,1,0:T(8,128)(2,1)}), bf16[8,48,256]{2,1,0:T(8,128)(2,1)S(1)}, u32[]{:S(2)}, u32[]{:S(2)}) async-start(bf16[8,48,256]{2,1,0:T(8,128)(2,1)} %reduce-scatter.2.cloned.1.call-done), calls=%async_computation.2 | async-start | bytes 393216 | tf_op jit(solution)/shard_map/all_to_all | solution.py:136
Sparse Core Ops, SparseCore 0:
  30.4 34.3 all-reduce.2
  89.3 21.2 reduce-scatter.1
where the time goes:
time: 133 us
  waiting for transfers between devices  62 us (47%)
  blocking collectives  20.7 us (16%)
  matrix products  19.3 us (15%)
  between operations  14.4 us (11%)
  other arithmetic  6.64 us (5%)
  starting transfers between devices  5.59 us (4%)
  local copies, waits for them, and re-layouts  4.08 us (3%)
    psum x1, waiting for transfers between devices, local(): lax.psum(partial_value.astype(jnp.bfloat16), 'tp').astype(jnp.float32)  33 us
    reduce_scatter x1, waiting for transfers between devices, local(): lax.psum_scatter(part_out.astype(jnp.bfloat16), 'tp', scatter_dimension=2...  21.5 us
    all_to_all x1, blocking collectives, local(): lax.all_to_all(buffer, 'ep', split_axis=0, concat_axis=0, tiled=True)  13.1 us
    all_gather x1, blocking collectives, local(): lax.all_gather(lax.all_to_all(buffer, 'ep', split_axis=0, concat_axis=0,...  7.58 us
    all_to_all x1, waiting for transfers between devices, local(): lax.all_to_all(shares, 'ep', split_axis=0, concat_axis=0, tiled=True)  7.57 us
    dot_general x1, matrix products, update_heads(): jnp.einsum('shvk,shk->shv', head_state, unit_key, precision=highest)  7.01 us
    all_to_all x1, starting transfers between devices, local(): lax.all_to_all(shares, 'ep', split_axis=0, concat_axis=0, tiled=True)  5.51 us
  transfers between devices with their start and end apart: 3, of which 3 were waited for; matrix products, arithmetic and copies ran while one was open for 1% of the time, Pallas kernels for 0%

commit v1 on v0

--- a/solution.py
+++ b/solution.py
@@ -8,6 +8,11 @@
 UNIT_EPS = 1e-06
 CLAMP_LIMIT = 7.0
 GLU_ALPHA = 1.702
+
+
+def stack_and_merge(array, name, dim):
+    tiles = lax.all_gather(array, name)
+    return jnp.concatenate(tiles, axis=dim)
 
 
 def row_norm(values):
@@ -116,11 +121,8 @@
         jnp.bfloat16
     )
     buffer = buffer.reshape(expert_count, capacity, outgoing.shape[1])
-    slot_rows = lax.all_gather(
-        lax.all_to_all(buffer, "ep", split_axis=0, concat_axis=0, tiled=True),
-        "tp",
-        axis=2,
-        tiled=True,
+    slot_rows = stack_and_merge(
+        lax.all_to_all(buffer, "ep", split_axis=0, concat_axis=0, tiled=True), "tp", 2
     )
     source_count, slot_count, model_width = slot_rows.shape
     flat_rows = slot_rows.reshape(-1, model_width)

time: 133 us -> 134 us (level)
  no operation moved by 1% of the time
where the time goes in v1:
time: 134 us
  waiting for transfers between devices  62 us (46%)
  blocking collectives  20.8 us (16%)
  matrix products  19.3 us (14%)
  between operations  14.4 us (11%)
  other arithmetic  6.64 us (5%)
  starting transfers between devices  5.59 us (4%)
  local copies, waits for them, and re-layouts  4.84 us (4%)
    psum x1, waiting for transfers between devices, local(): lax.psum(partial_value.astype(jnp.bfloat16), 'tp').astype(jnp.float32)  33 us
    reduce_scatter x1, waiting for transfers between devices, local(): lax.psum_scatter(part_out.astype(jnp.bfloat16), 'tp', scatter_dimension=2...  21.5 us
    all_to_all x1, blocking collectives, local(): lax.all_to_all(buffer, 'ep', split_axis=0, concat_axis=0, tiled=True)  13.2 us
    all_gather x1, blocking collectives, stack_and_merge(): tiles = lax.all_gather(array, name)  7.58 us
    all_to_all x1, waiting for transfers between devices, local(): lax.all_to_all(shares, 'ep', split_axis=0, concat_axis=0, tiled=True)  7.57 us
    dot_general x1, matrix products, update_heads(): jnp.einsum('shvk,shk->shv', head_state, unit_key, precision=highest)  7.01 us
    all_to_all x1, starting transfers between devices, local(): lax.all_to_all(shares, 'ep', split_axis=0, concat_axis=0, tiled=True)  5.51 us
  transfers between devices with their start and end apart: 3, of which 3 were waited for; matrix products, arithmetic and copies ran while one was open for 1% of the time, Pallas kernels for 0%

profile of v1, /device:TPU:0, one launch (start us, length us, event | category | flops | bytes accessed | tf_op | source)
XLA Modules:
  0.0 133.6 jit_solution(3989017997268242690)
XLA Ops:
  7.2 1.1 fusion.22
  8.3 1.2 fusion.10
  9.8 1.3 fusion.6
  11.2 1.4 %fusion.35 = f32[48,128]{1,0:T(8,128)S(1)} fusion(bf16[64,128]{1,0:T(8,128)(2,1)} %param.24, bf16[1024,64]{0,1:T(8,128)(2,1)} %param.23, f32[128]{0:T(128)} %param.25, bf16[48,1024]{1,0:T(8,128)(2,1)} %param.18, f32[48]{0:T(128)S(1)} %add_rsqrt_fusion.3), kind=kOutput, calls=%fused_computation.59 | convolution fusion | flops 7296000 | bytes 271040 | tf_op jit(solution)/shard_map/dot_general | solution.py:88
  12.7 1.2 fusion.9
  14.0 1.2 convolution_convert_fusion.3
  15.5 7.0 %fusion.55 = f32[48,2,1,64]{3,2,1,0:T(1,128)S(1)} fusion(f32[48,2,64,1]{2,3,1,0:T(1,128)S(1)} %bitcast.60, f32[48,2,64,64]{3,2,1,0:T(8,128)} %param.19), kind=kOutput, calls=%fused_computation.87 | convolution fusion | flops 4718592 | bytes 1622016 | tf_op jit(solution)/shard_map/shvk,shk->shv/dot_general | solution.py:43
  22.5 2.1 %multiply_add_fusion = f32[48,2,64,64]{3,2,1,0:T(8,128)S(1)} fusion(f32[48,2,64,64]{3,2,1,0:T(8,128)S(1)} %copy-done.1, f32[48,2,64]{2,1,0:T(2,128)S(1)} %get-tuple-element.6, f32[48,2,64]{2,1,0:T(2,128)S(1)} %reshape.152, f32[48,2,64]{2,1,0:T(2,128)S(1)} %get-tuple-element.4, f32[48,2,64]{2,1,0:T(2,128)S(1)} %bitcast.59, f32[48,2,64]{2,1,0:T(2,128)S(1)} %mul.155), kind=kLoop, calls=%fused_computation.1 | loop fusion | flops 1966080 | bytes 3268608 | tf_op jit(solution)/shard_map/add | solution.py:45
  24.6 1.7 %copy-done.2 = f32[48,2,64,64]{3,2,1,0:T(8,128)} copy-done((f32[48,2,64,64]{3,2,1,0:T(8,128)}, f32[48,2,64,64]{3,2,1,0:T(8,128)S(1)}, u32[]{:S(2)}) %copy-start.2) | copy-done | bytes 1572888
  26.2 2.5 %fusion.56 = f32[48,2,1,64]{3,2,1,0:T(1,128)S(1)} fusion(f32[48,2,64,64]{3,2,1,0:T(8,128)S(1)} %multiply_add_fusion, bf16[48,2,64,1]{2,3,1,0:T(2,128)(2,1)S(1)} %reshape.169), kind=kOutput, calls=%fused_computation.88 | convolution fusion | flops 4718592 | bytes 1609728 | tf_op jit(solution)/shard_map/shvk,shk->shv/dot_general | solution.py:49
  29.4 0.8 convolution_convert_fusion.2
  30.6 0.6 reduce-window.6
  31.8 33.0 %all-reduce.3.cloned.1.call-done = bf16[48,1024]{1,0:T(8,128)(2,1)} async-done(((bf16[48,1024]{1,0:T(8,128)(2,1)}), bf16[48,1024]{1,0:T(8,128)(2,1)}) %all-reduce.3.cloned.1.call-update) | async-done | bytes 98320 | tf_op jit(solution)/shard_map/psum | solution.py:100
  64.8 1.0 multiply_reduce_fusion.1
  66.2 13.2 %all_to_all.10 = bf16[8,48,256]{2,1,0:T(8,128)(2,1)S(1)} all-to-all(bf16[8,48,256]{2,1,0:T(8,128)(2,1)S(1)} %bitcast.55), channel_id=1, replica_groups=mesh['ep'=8,'tp'=4] {'ep'}, dimensions={0} | all-to-all | bytes 393216 | tf_op jit(solution)/shard_map/all_to_all | solution.py:125
  79.4 7.6 %all-gather = bf16[32,48,256]{2,1,0:T(8,128)(2,1)S(1)} all-gather(bf16[8,48,256]{2,1,0:T(8,128)(2,1)S(1)} %all_to_all.10), channel_id=2, replica_groups=mesh['ep'=8,'tp'=4] {'tp'}, dimensions={0}, use_global_device_ids=true | all-gather | bytes 983040 | tf_op jit(solution)/shard_map/all_gather | solution.py:14
  87.0 0.6 copy.46
  87.8 0.4 convolution_minimum_fusion
  88.2 1.9 %convolution_convert_fusion = bf16[384,1024]{1,0:T(8,128)(2,1)} fusion(bf16[384,1024]{1,0:T(8,128)(2,1)S(1)} %bitcast.52, bf16[1,256,1024]{2,1,0:T(8,128)(2,1)S(1)} %copy-done, bf16[1,1024,256]{2,1,0:T(8,128)(2,1)S(1)} %copy-done.9, f32[384,256]{1,0:T(8,128)S(1)} %convolution_minimum_fusion), kind=kOutput, calls=%fused_computation.2 | convolution fusion | flops 403931136 | bytes 3014656 | tf_op jit(solution)/shard_map/dot_general | solution.py:132
  90.1 21.5 %reduce-scatter.2.cloned.1.call-done = bf16[8,48,256]{2,1,0:T(8,128)(2,1)} async-done(((bf16[8,48,1024]{2,1,0:T(8,128)(2,1)}), bf16[8,48,256]{2,1,0:T(8,128)(2,1)}) %reduce-scatter.2.cloned.1.call-update) | async-done | bytes 196624 | tf_op jit(solution)/shard_map/reduce_scatter | solution.py:137
  111.6 5.5 %all-to-all-start.1 = ((bf16[8,48,256]{2,1,0:T(8,128)(2,1)}), bf16[8,48,256]{2,1,0:T(8,128)(2,1)S(1)}, u32[]{:S(2)}, u32[]{:S(2)}) async-start(bf16[8,48,256]{2,1,0:T(8,128)(2,1)} %reduce-scatter.2.cloned.1.call-done), calls=%async_computation.2 | async-start | bytes 393216 | tf_op jit(solution)/shard_map/all_to_all | solution.py:138
  117.3 7.6 %all-to-all-done.1 = bf16[8,48,256]{2,1,0:T(8,128)(2,1)S(1)} async-done(((bf16[8,48,256]{2,1,0:T(8,128)(2,1)}), bf16[8,48,256]{2,1,0:T(8,128)(2,1)S(1)}, u32[]{:S(2)}, u32[]{:S(2)}) %all-to-all-start.1) | async-done | bytes 196640 | tf_op jit(solution)/shard_map/all_to_all | solution.py:138
  124.9 1.0 gather_fusion
  126.1 0.6 add_convert_fusion
  (61 shorter events, 3.3 us)
Async XLA Ops:
  7.2 81.0 %copy-start = (bf16[1,256,1024]{2,1,0:T(8,128)(2,1)S(1)}, bf16[1,256,1024]{2,1,0:T(8,128)(2,1)}, u32[]{:S(2)}) copy-start(bf16[1,256,1024]{2,1,0:T(8,128)(2,1)} %param.35) | copy-start | bytes 1572868
  7.2 57.6 %all-reduce.3.cloned.1.call-start = ((), (), s32[]{:S(2)}) async-start(), calls=%async_computation.3 | async-start | bytes 196608 | tf_op jit(solution)/shard_map/psum | solution.py:100
  15.3 7.2 %copy-start.1 = (f32[48,2,64,64]{3,2,1,0:T(8,128)S(1)}, f32[48,2,64,64]{3,2,1,0:T(8,128)}, u32[]{:S(2)}) copy-start(f32[48,2,64,64]{3,2,1,0:T(8,128)} %param.19) | copy-start | bytes 4718596
  24.6 1.7 %copy-start.2 = (f32[48,2,64,64]{3,2,1,0:T(8,128)}, f32[48,2,64,64]{3,2,1,0:T(8,128)S(1)}, u32[]{:S(2)}) copy-start(f32[48,2,64,64]{3,2,1,0:T(8,128)S(1)} %multiply_add_fusion) | copy-start | bytes 4718596
  26.2 3.2 %copy-start.5 = (bf16[128,1024]{1,0:T(8,128)(2,1)S(1)}, bf16[128,1024]{1,0:T(8,128)(2,1)}, u32[]{:S(2)}) copy-start(bf16[128,1024]{1,0:T(8,128)(2,1)} %param.30) | copy-start | bytes 786436
  26.2 3.2 %copy-start.8 = (f32[128]{0:T(128)S(1)}, f32[128]{0:T(128)}, u32[]{:S(2)}) copy-start(f32[128]{0:T(128)} %param.29) | copy-start | bytes 1540
  26.2 4.1 %copy-start.6 = (s32[48,4]{0,1:T(4,128)S(1)}, s32[48,4]{0,1:T(4,128)}, u32[]{:S(2)}) copy-start(s32[48,4]{0,1:T(4,128)} %param.31) | copy-start | bytes 2308
  26.2 38.6 %copy-start.3 = (bf16[48,1024]{1,0:T(8,128)(2,1)S(1)}, bf16[48,1024]{1,0:T(8,128)(2,1)}, u32[]{:S(2)}) copy-start(bf16[48,1024]{1,0:T(8,128)(2,1)} %param.18) | copy-start | bytes 294916
  29.3 58.5 %copy-start.4 = (bf16[1,1024,256]{2,1,0:T(8,128)(2,1)S(1)}, bf16[1,1024,256]{2,1,0:T(8,128)(2,1)}, u32[]{:S(2)}) copy-start(bf16[1,1024,256]{2,1,0:T(8,128)(2,1)} %param.33) | copy-start | bytes 1572868
  30.3 81.3 %reduce-scatter.2.cloned.1.call-start = ((), (), s32[]{:S(2)}) async-start(), calls=%async_computation.4 | async-start | bytes 983040 | tf_op jit(solution)/shard_map/reduce_scatter | solution.py:137
  66.2 22.0 %copy-start.9 = (bf16[1,1024,256]{2,1,0:T(8,128)(2,1)S(1)}, bf16[1,1024,256]{2,1,0:T(8,128)(2,1)}, u32[]{:S(2)}) copy-start(bf16[1,1024,256]{2,1,0:T(8,128)(2,1)} %param.34) | copy-start | bytes 1572868
  88.2 29.0 %copy-start.7 = (f32[48,4]{0,1:T(4,128)S(1)}, f32[48,4]{0,1:T(4,128)}, u32[]{:S(2)}) copy-start(f32[48,4]{0,1:T(4,128)} %param.32) | copy-start | bytes 2308
  111.6 13.3 %all-to-all-start.1 = ((bf16[8,48,256]{2,1,0:T(8,128)(2,1)}), bf16[8,48,256]{2,1,0:T(8,128)(2,1)S(1)}, u32[]{:S(2)}, u32[]{:S(2)}) async-start(bf16[8,48,256]{2,1,0:T(8,128)(2,1)} %reduce-scatter.2.cloned.1.call-done), calls=%async_computation.2 | async-start | bytes 393216 | tf_op jit(solution)/shard_map/all_to_all | solution.py:138
Sparse Core Ops, SparseCore 0:
  30.4 34.3 all-reduce.2
  90.2 21.2 reduce-scatter.1
